TPU v7x, 128 devices: a whole 4x4x4 slice. The times are simulated.
128 devices in a mesh: sp: 16 (over z, y), dp: 8 (over x, core).
Axes of the slice: x: 4, y: 4, z: 4, core: 2. Of those that a mesh axis runs over, the one named last changes fastest.
Arguments:
- query_first: bfloat16 [8, 2048, 1024], P('dp', 'sp'), may hold values from -200 to 200
- key_first: bfloat16 [8, 2048, 1024], P('dp', 'sp'), may hold values from -8 to 8
- query_second: bfloat16 [8, 2048, 1024], P('dp', 'sp'), may hold values from -200 to 200
- key_second: bfloat16 [8, 2048, 1024], P('dp', 'sp'), may hold values from -8 to 8
- value_rows: bfloat16 [8, 2048, 2048], P('dp', 'sp'), may hold values from -6 to 6
- mix_lambda: float32 [16], replicated, may hold values from 0.3 to 0.8
- head_gain: float32 [128], replicated, may hold values from 0.1 to 1.9
- residual: bfloat16 [8, 2048, 2048], P('dp', 'sp'), may hold values from -6 to 6
- out_weight: bfloat16 [2048, 2048], replicated, may hold values from -0.125 to 0.125
- norm_gain: float32 [2048], replicated, may hold values from 0.1 to 1.9
- routes: int32 [8, 2048, 4], P('dp', 'sp'), may hold values from 0 to 127, all different within a row; in each aligned block of 128 rows (0 to 127, 128 to 255, ..., all dimensions but the last counted through in order) at most 6 rows name the same one
- route_weights: float32 [8, 2048, 4], P('dp', 'sp'), may hold values from 0.1 to 1
- gate_weight: bfloat16 [128, 2048, 1024], P(('sp', 'dp')), may hold values from -0.375 to 0.375
- up_weight: bfloat16 [128, 2048, 1024], P(('sp', 'dp')), may hold values from -0.375 to 0.375
- down_weight: bfloat16 [128, 1024, 2048], P(('sp', 'dp')), may hold values from -0.046875 to 0.046875
Outputs:
- layer_out: bfloat16 [8, 2048, 2048], P('dp', 'sp')
Inputs may be any that keep to these rules, and one draw needn't show every extreme that they name: `routes`: within the rows of one device (aligned blocks of 128 positions of a sequence) no expert is named more than 6 times, a bound that some block reaches.
All inputs are finite; a program needn't handle non-finite values.
Results may differ from a plain program's by a relative error of at most 0.0075.
Values may be sent and summed in bfloat16 or wider, within the bound.
A program may use at most 128 MiB of HBM per device.

v0:
```python
import functools
import jax
import jax.numpy as jnp
from jax import lax
from jax.experimental import pallas as pl
from jax.experimental.pallas import tpu as pltpu
from jax.sharding import PartitionSpec as P

MESH = pl.DeviceIdType.MESH
RING = 4
CAP = 6
OFFSETS = (
    (0, 1), (1, 0), (0, 3), (3, 0), (1, 1), (3, 3), (1, 3), (3, 1),
    (0, 2), (2, 0), (1, 2), (2, 1), (3, 2), (2, 3), (2, 2),
)
CHUNKS = 4


def moe_kernel(
    head_ref, res_ref, wo_hbm, gain_ref, meta_ref, wg_hbm, wu_hbm, wd_hbm,
    out_ref,
    wg, wu, wd, nrm, mixed, gath, slab, xin, gacc, uacc, hid, back, rin,
    part_out, part_in, sum_out, sum_in, own, pick, wsel, meta,
    wsem, meta_s, meta_r, xs, xr, cs, cr, ds, dr, bs, br, ps, pr, ts, tr,
):
    f32, bf16 = jnp.float32, jnp.bfloat16
    sp, dp = lax.axis_index("sp"), lax.axis_index("dp")
    z, y = sp // RING, sp % RING
    x, c = dp // 2, dp % 2
    partner = x * 2 + (1 - c)
    rows, width = res_ref.shape
    n = CHUNKS
    cw = width // n
    slots = slab.shape[1]
    nsp = slab.shape[0]
    ndp = gath.shape[0]
    half = wg.shape[1]

    def cols(k):
        return pl.ds(pl.multiple_of(k * cw, cw), cw)

    def peer(i, sign=1):
        dz, dy = OFFSETS[i]
        return ((z + sign * dz + RING) % RING) * RING + (y + sign * dy + RING) % RING

    def xpeer(i, sign=1):
        return (x + sign * (i + 1) + RING) % RING

    def remote(src, dst, ssem, rsem, to):
        return pltpu.make_async_remote_copy(
            src_ref=src, dst_ref=dst, send_sem=ssem, recv_sem=rsem,
            device_id=to, device_id_type=MESH,
        )

    barrier = pltpu.get_barrier_semaphore()
    for i in range(nsp - 1):
        pl.semaphore_signal(barrier, inc=1, device_id=(peer(i), dp), device_id_type=MESH)
    for i in range(1, ndp):
        pl.semaphore_signal(barrier, inc=1, device_id=(sp, (dp + i) % ndp), device_id_type=MESH)

    wo_a = pltpu.make_async_copy(wo_hbm.at[:, pl.ds(0, half)], wg, wsem.at[0])
    wo_b = pltpu.make_async_copy(wo_hbm.at[:, pl.ds(half, half)], wu, wsem.at[1])
    wd_c = pltpu.make_async_copy(wd_hbm, wd, wsem.at[2])
    wg_c = pltpu.make_async_copy(wg_hbm, wg, wsem.at[3])
    wu_c = pltpu.make_async_copy(wu_hbm, wu, wsem.at[4])
    wo_a.start()
    wo_b.start()
    wd_c.start()

    pl.semaphore_wait(barrier, nsp - 1 + ndp - 1)

    def meta_copy(i, src):
        return remote(meta_ref, meta.at[src], meta_s.at[i], meta_r.at[i], (sp, (dp + i) % ndp))

    for i in range(1, ndp):
        meta_copy(i, dp).start()
    meta[dp] = meta_ref[...]

    tile = 256
    square = jnp.zeros((rows, 128), f32)

    def project(weights, base, t, total):
        at = pl.ds(pl.multiple_of(t * tile, tile), tile)
        to = pl.ds(pl.multiple_of(base + t * tile, tile), tile)
        value = jnp.dot(head_ref[...], weights[:, at], preferred_element_type=f32)
        value = value + res_ref[:, to].astype(f32)
        mixed[:, to] = value
        sq = value * value
        return total + sq[:, :128] + sq[:, 128:]

    wo_a.wait()
    square = lax.fori_loop(0, half // tile, lambda t, v: project(wg, 0, t, v), square)
    wg_c.start()
    wo_b.wait()
    square = lax.fori_loop(0, half // tile, lambda t, v: project(wu, half, t, v), square)
    wu_c.start()
    factor = lax.rsqrt(jnp.sum(square, axis=1, keepdims=True) / width + 1e-06)

    def gx(k, i, src):
        return remote(
            nrm.at[:, cols(k)], gath.at[src * 2 + c, :, cols(k)], xs.at[k, i], xr.at[k, i],
            (sp, xpeer(i) * 2 + c),
        )

    def gown(k):
        return remote(
            nrm.at[:, cols(k)], gath.at[dp, :, cols(k)], cs.at[k, 3], cr.at[k, 3], (sp, partner)
        )

    def gfwd(k, i, core):
        at = (xpeer(i, -1) * 2 + core)
        return remote(
            gath.at[at, :, cols(k)], gath.at[at, :, cols(k)], cs.at[k, i], cr.at[k, i],
            (sp, partner),
        )

    def gsend(k):
        for i in (0, 2, 1):
            gx(k, i, x).start()
        gown(k).start()

    for k in range(n):
        nrm[:, cols(k)] = (mixed[:, cols(k)] * factor * gain_ref[:, cols(k)]).astype(bf16)
        if k > 0:
            gsend(k - 1)
    gath[dp] = nrm[...]
    gsend(n - 1)

    for i in range(1, ndp):
        meta_copy(i, (dp - i + ndp) % ndp).wait_recv()
    before = (
        lax.broadcasted_iota(jnp.int32, (rows, rows), 0)
        < lax.broadcasted_iota(jnp.int32, (rows, rows), 1)
    ).astype(bf16)
    expert = (lax.broadcasted_iota(jnp.int32, (nsp, rows), 0) * ndp + dp).astype(f32)
    place = lax.broadcasted_iota(jnp.int32, (nsp, slots, rows), 1).astype(f32)

    def table(b, carry):
        info = meta[b]
        named = jnp.zeros((nsp, rows), f32)
        weight = jnp.zeros((nsp, rows), f32)
        for t in range(RING):
            hit = (info[t : t + 1, :] == expert).astype(f32)
            named = named + hit
            weight = weight + hit * info[t + RING : t + RING + 1, :]
        rank = jnp.dot(named.astype(bf16), before, preferred_element_type=f32)
        slot = jnp.where(named > 0.0, rank + (b * CAP).astype(f32), -1.0)
        match = (slot[:, None, :] == place).astype(f32)
        at = pl.ds(pl.multiple_of(b * rows, rows), rows)
        pick[:, at] = match.reshape(nsp * slots, rows).astype(bf16)
        scaled = (match * weight[:, None, :]).reshape(nsp * slots, rows)
        wsel[(b % 2) * RING + b // 2] = jnp.transpose(scaled).astype(bf16)
        return carry

    lax.fori_loop(0, ndp, table, 0)
    gacc[...] = jnp.zeros_like(gacc)
    uacc[...] = jnp.zeros_like(uacc)

    def forward(k):
        for i in (0, 2, 1):
            gx(k, i, xpeer(i, -1)).wait_recv()
            gfwd(k, i, c).start()

    def exchange(out_buf, in_buf, ssem, rsem, k, i, src, dst):
        return remote(
            out_buf.at[dst, :, cols(k)], in_buf.at[src, :, cols(k)], ssem.at[k, i], rsem.at[k, i],
            (dst, dp),
        )

    def send_all(out_buf, in_buf, ssem, rsem, k):
        for i in range(nsp - 1):
            exchange(out_buf, in_buf, ssem, rsem, k, i, sp, peer(i)).start()

    def wait_all(out_buf, in_buf, ssem, rsem, k):
        for i in range(nsp - 1):
            exchange(out_buf, in_buf, ssem, rsem, k, i, peer(i, -1), peer(i)).wait_recv()

    def build(k):
        for i in range(3):
            gfwd(k, i, 1 - c).wait_recv()
        remote(
            nrm.at[:, cols(k)], gath.at[partner, :, cols(k)], cs.at[k, 3], cr.at[k, 3], (sp, partner)
        ).wait_recv()
        tokens = gath[:, :, cols(k)].reshape(ndp * rows, cw)
        group = nsp // 4

        def one(g, carry):
            sel = pick[pl.ds(pl.multiple_of(g * group * slots, group * slots), group * slots), :]
            made = jnp.dot(sel, tokens, preferred_element_type=f32).astype(bf16)
            slab[pl.ds(g * group, group), :, cols(k)] = made.reshape(group, slots, cw)
            return carry

        lax.fori_loop(0, 4, one, 0)
        xin[sp, :, cols(k)] = slab[sp, :, cols(k)]

    def expert_in(k):
        wait_all(slab, xin, ds, dr, k)

        def one(t, carry):
            at = pl.ds(pl.multiple_of(t * tile, tile), tile)
            taken = xin[:, :, cols(k)].reshape(nsp * slots, cw)
            gacc[:, at] += jnp.dot(taken, wg[cols(k), at], preferred_element_type=f32)
            uacc[:, at] += jnp.dot(taken, wu[cols(k), at], preferred_element_type=f32)
            return carry

        lax.fori_loop(0, half // tile, one, 0)

    forward(0)

    def dispatch(k, carry):
        build(k)
        send_all(slab, xin, ds, dr, k)

        @pl.when(k + 1 < n)
        def _():
            forward(k + 1)

        @pl.when(k == 1)
        def _():
            wg_c.wait()
            wu_c.wait()

        @pl.when(k > 0)
        def _():
            expert_in(k - 1)

        return carry

    lax.fori_loop(0, n, dispatch, 0)
    expert_in(n - 1)

    def unit(t, carry):
        at = pl.ds(pl.multiple_of(t * 32, 32), 32)
        gate = jnp.minimum(gacc[at, :], 7.0)
        upper = jnp.clip(uacc[at, :], -7.0, 7.0) + 1.0
        hid[at, :] = (upper * gate / (1.0 + jnp.exp(-1.702 * gate))).astype(bf16)
        return carry

    lax.fori_loop(0, nsp * slots // 32, unit, 0)
    wd_c.wait()

    def down(k, carry):
        def one(t, inner):
            at = pl.ds(pl.multiple_of(k * cw + t * tile, tile), tile)
            made = jnp.dot(hid[...], wd[:, at], preferred_element_type=f32).astype(bf16)
            back[:, :, at] = made.reshape(nsp, slots, tile)
            return inner

        lax.fori_loop(0, cw // tile, one, 0)
        rin[sp, :, cols(k)] = back[sp, :, cols(k)]
        send_all(back, rin, bs, br, k)
        return carry

    lax.fori_loop(0, n, down, 0)

    def part(k):
        return remote(
            part_out.at[:, :, cols(k)], part_in.at[:, :, cols(k)], ps.at[k], pr.at[k], (sp, partner)
        )

    def total(k, i, src):
        return remote(
            sum_out.at[xpeer(i), :, cols(k)], sum_in.at[src, :, cols(k)], ts.at[k, i], tr.at[k, i],
            (sp, xpeer(i) * 2 + c),
        )

    def weighted(core, k):
        sel = wsel[pl.ds(core * RING, RING)].reshape(RING * rows, nsp * slots)
        taken = rin[:, :, cols(k)].reshape(nsp * slots, cw)
        return jnp.dot(sel, taken, preferred_element_type=f32).reshape(RING, rows, cw)

    def finish(k):
        value = mixed[:, cols(k)]
        for i in range(3):
            total(k, i, xpeer(i, -1)).wait_recv()
            value = value + sum_in[xpeer(i, -1), :, cols(k)].astype(f32)
        out_ref[:, cols(k)] = value.astype(bf16)

    def combine(k, carry):
        wait_all(back, rin, bs, br, k)
        part_out[:, :, cols(k)] = weighted(1 - c, k).astype(bf16)
        own[...] = weighted(c, k)
        part(k).start()
        part(k).wait_recv()
        mixed[:, cols(k)] += own[x] + part_in[x, :, cols(k)].astype(f32)
        sum_out[:, :, cols(k)] = (own[...] + part_in[:, :, cols(k)].astype(f32)).astype(bf16)
        for i in (1, 0, 2):
            total(k, i, x).start()

        @pl.when(k > 0)
        def _():
            finish(k - 1)

        return carry

    lax.fori_loop(0, n, combine, 0)
    finish(n - 1)

    for i in range(1, ndp):
        meta_copy(i, dp).wait_send()

    def drain(k, carry):
        for i in range(3):
            gx(k, i, x).wait_send()
            gfwd(k, i, c).wait_send()
            total(k, i, x).wait_send()
        gown(k).wait_send()
        part(k).wait_send()
        for i in range(nsp - 1):
            exchange(slab, xin, ds, dr, k, i, sp, peer(i)).wait_send()
            exchange(back, rin, bs, br, k, i, sp, peer(i)).wait_send()
        return carry

    lax.fori_loop(0, n, drain, 0)


def after_attention(heads_out, residual, out_weight, norm_gain, meta, gate_weight, up_weight, down_weight, nsp, ndp):
    rows, width = residual.shape
    hidden = gate_weight.shape[1]
    slots = CAP * ndp
    n = CHUNKS
    bf16, f32 = jnp.bfloat16, jnp.float32
    vmem = pl.BlockSpec(memory_space=pltpu.VMEM)
    hbm = pl.BlockSpec(memory_space=pl.ANY)
    dma = pltpu.SemaphoreType.DMA
    return pl.pallas_call(
        moe_kernel,
        out_shape=jax.ShapeDtypeStruct((rows, width), bf16),
        in_specs=[vmem, vmem, hbm, vmem, vmem, hbm, hbm, hbm],
        out_specs=vmem,
        scratch_shapes=[
            pltpu.VMEM((width, hidden), bf16),
            pltpu.VMEM((width, hidden), bf16),
            pltpu.VMEM((hidden, width), bf16),
            pltpu.VMEM((rows, width), bf16),
            pltpu.VMEM((rows, width), f32),
            pltpu.VMEM((ndp, rows, width), bf16),
            pltpu.VMEM((nsp, slots, width), bf16),
            pltpu.VMEM((nsp, slots, width), bf16),
            pltpu.VMEM((nsp * slots, hidden), f32),
            pltpu.VMEM((nsp * slots, hidden), f32),
            pltpu.VMEM((nsp * slots, hidden), bf16),
            pltpu.VMEM((nsp, slots, width), bf16),
            pltpu.VMEM((nsp, slots, width), bf16),
            pltpu.VMEM((RING, rows, width), bf16),
            pltpu.VMEM((RING, rows, width), bf16),
            pltpu.VMEM((RING, rows, width), bf16),
            pltpu.VMEM((RING, rows, width), bf16),
            pltpu.VMEM((RING, rows, width // n), f32),
            pltpu.VMEM((nsp * slots, ndp * rows), bf16),
            pltpu.VMEM((ndp, rows, nsp * slots), bf16),
            pltpu.VMEM((ndp, 8, rows), f32),
            dma((5,)), dma((ndp,)), dma((ndp,)),
            dma((n, 3)), dma((n, 3)), dma((n, 4)), dma((n, 4)),
            dma((n, nsp)), dma((n, nsp)), dma((n, nsp)), dma((n, nsp)),
            dma((n,)), dma((n,)), dma((n, 3)), dma((n, 3)),
        ],
        compiler_params=pltpu.CompilerParams(
            collective_id=1, has_side_effects=True, vmem_limit_bytes=64 * 1000 * 1000
        ),
        name="experts",
    )(heads_out, residual, out_weight, norm_gain[None, :], meta, gate_weight, up_weight, down_weight)


def sent_together(arrays, axis, split_dim, concat_dim, along):
    widths = [a.shape[along] for a in arrays]
    both = jnp.concatenate(arrays, axis=along)
    out = lax.all_to_all(both, axis, split_axis=split_dim, concat_axis=concat_dim, tiled=True)
    return tuple(jnp.split(out, [sum(widths[:k]) for k in range(1, len(widths))], axis=along))


def on_device(
    query_first,
    key_first,
    query_second,
    key_second,
    value_rows,
    mix_lambda,
    head_gain,
    residual,
    out_weight,
    norm_gain,
    routes,
    route_weights,
    gate_weight,
    up_weight,
    down_weight,
):
    tok_rows = query_first.shape[1]
    heads = mix_lambda.shape[0]
    query_one, key_one, query_two, key_two, value_head = sent_together(
        (
            query_first[0].reshape(tok_rows, heads, -1),
            key_first[0].reshape(tok_rows, heads, -1),
            query_second[0].reshape(tok_rows, heads, -1),
            key_second[0].reshape(tok_rows, heads, -1),
            value_rows[0].reshape(tok_rows, heads, -1),
        ),
        "sp",
        1,
        0,
        2,
    )
    length = query_one.shape[0]
    local = query_one.shape[1]
    value_width = value_head.shape[2]
    scale = query_one.shape[2] ** (-0.5)
    first_head = lax.axis_index("sp") * local
    weight_two = lax.dynamic_slice_in_dim(mix_lambda, first_head, local)[:, None, None]
    qblock = min(length, max(512, length // 16))
    outputs = []
    for step in range(length // qblock):
        begin = step * qblock
        finish = begin + qblock
        score_one = (
            jnp.einsum(
                "qhd,khd->hqk",
                query_one[begin:finish],
                key_one[:finish],
                preferred_element_type=jnp.float32,
            )
            * scale
        )
        score_two = (
            jnp.einsum(
                "qhd,khd->hqk",
                query_two[begin:finish],
                key_two[:finish],
                preferred_element_type=jnp.float32,
            )
            * scale
        )
        visible = jnp.arange(finish)[None, :] <= (begin + jnp.arange(qblock))[:, None]
        prob_one = jax.nn.softmax(jnp.where(visible[None], score_one, -1e30), axis=-1)
        prob_two = jax.nn.softmax(jnp.where(visible[None], score_two, -1e30), axis=-1)
        mixture = (prob_one - weight_two * prob_two).astype(jnp.bfloat16)
        head_raw = jnp.einsum(
            "hqk,khe->qhe", mixture, value_head[:finish], preferred_element_type=jnp.float32
        )
        factor = lax.rsqrt(jnp.mean(head_raw * head_raw, axis=-1, keepdims=True) + 1e-06)
        outputs.append((head_raw * factor * head_gain).astype(jnp.bfloat16))
    head_out = jnp.concatenate(outputs, axis=0)
    returned = lax.all_to_all(head_out, "sp", split_axis=0, concat_axis=1, tiled=True)
    meta = jnp.concatenate([routes[0].T.astype(jnp.float32), route_weights[0].T], axis=0)
    out = after_attention(
        returned.reshape(tok_rows, heads * value_width),
        residual[0],
        out_weight,
        norm_gain,
        meta,
        gate_weight[0],
        up_weight[0],
        down_weight[0],
        lax.axis_size("sp"),
        lax.axis_size("dp"),
    )
    return out[None]


def solution(mesh):
    return jax.shard_map(
        on_device,
        mesh=mesh,
        in_specs=(
            P("dp", "sp", None),
            P("dp", "sp", None),
            P("dp", "sp", None),
            P("dp", "sp", None),
            P("dp", "sp", None),
            P(),
            P(),
            P("dp", "sp", None),
            P(),
            P(),
            P("dp", "sp", None),
            P("dp", "sp", None),
            P(("sp", "dp"), None, None),
            P(("sp", "dp"), None, None),
            P(("sp", "dp"), None, None),
        ),
        out_specs=P("dp", "sp", None),
        check_vma=False,
    )
```

profile of v0, /device:TPU:9, one launch (start us, length us, event | category | flops | bytes accessed | tf_op | source)
XLA Modules:
  0.0 193.5 jit_solution(12563747857431201436)
XLA Ops:
  0.0 0.0 copy-start.1
  0.0 0.0 copy-start
  0.0 1.2 copy.89
  1.2 0.8 constant_dynamic-update-slice_fusion.4
  2.0 1.1 copy.90
  3.1 1.1 copy.91
  4.2 0.0 copy-done.1
  4.2 0.2 copy.92
  4.4 0.0 copy-done
  4.4 0.3 copy.93
  4.7 0.8 constant_dynamic-update-slice_fusion.3
  5.5 0.8 constant_dynamic-update-slice_fusion.2
  6.2 0.8 constant_dynamic-update-slice_fusion.1
  7.0 0.0 copy-start.5
  7.0 0.9 constant_dynamic-update-slice_fusion
  7.9 7.8 %all-to-all-start = ((bf16[128,16,384]{0,2,1:T(8,128)(2,1)}), bf16[128,16,384]{0,2,1:T(8,128)(2,1)S(1)}, u32[]{:S(2)}, u32[]{:S(2)}) async-start(bf16[128,16,384]{0,2,1:T(8,128)(2,1)} %constant_dynamic-update-slice_fusion), calls=%async_computation | async-start | bytes 3145728 | tf_op jit(solution)/shard_map/all_to_all | solution.py:368
  15.7 0.0 copy-done.5
  15.7 0.6 dynamic_slice.3
  16.3 20.0 %all-to-all-done = bf16[128,16,384]{0,2,1:T(8,128)(2,1)S(1)} async-done(((bf16[128,16,384]{0,2,1:T(8,128)(2,1)}), bf16[128,16,384]{0,2,1:T(8,128)(2,1)S(1)}, u32[]{:S(2)}, u32[]{:S(2)}) %all-to-all-start) | async-done | bytes 1572896 | tf_op jit(solution)/shard_map/all_to_all | solution.py:368
  36.3 0.9 copy.94
  37.2 1.0 fusion.26
  38.2 1.0 fusion.27
  39.2 0.8 fusion.24
  40.1 0.8 fusion.25
  40.9 0.7 fusion.22
  41.6 0.7 fusion.23
  42.3 0.4 fusion.20
  42.6 0.4 fusion.21
  43.0 1.3 fusion
  44.3 2.7 %multiply_reduce_fusion = (f32[512]{0:T(512)S(1)}, f32[1,128,512]{2,1,0:T(8,128)S(1)}) fusion(f32[512,2048]{1,0:T(8,128)S(1)} %get-tuple-element.30, f32[512,2048]{1,0:T(8,128)S(1)} %get-tuple-element.28, f32[512]{0:T(512)S(1)} %get-tuple-element.40, f32[512]{0:T(512)S(1)} %get-tuple-element.27, f32[]{:T(128)} %bitcast.11, f32[512]{0:T(512)S(1)} %get-tuple-element.39, ...), kind=kOutput, calls=%fused_computation.54 | convolution fusion | flops 275906048 | bytes 9185284 | tf_op jit(solution)/shard_map/hqk,khe->qhe/dot_general | solution.py:437
  47.0 1.0 fusion.4
  48.0 2.2 %multiply_reduce_fusion.1 = (f32[512]{0:T(512)S(1)}, f32[1,128,512]{2,1,0:T(8,128)S(1)}) fusion(f32[512,1536]{1,0:T(8,128)S(1)} %get-tuple-element.24, f32[512,1536]{1,0:T(8,128)S(1)} %get-tuple-element.22, f32[512]{0:T(512)S(1)} %get-tuple-element.38, f32[512]{0:T(512)S(1)} %get-tuple-element.21, f32[]{:T(128)} %bitcast.11, f32[512]{0:T(512)S(1)} %get-tuple-element.37, ...), kind=kOutput, calls=%fused_computation.56 | convolution fusion | flops 206962176 | bytes 6957060 | tf_op jit(solution)/shard_map/hqk,khe->qhe/dot_general | solution.py:437
  50.2 1.1 fusion.7
  51.3 2.0 %multiply_reduce_fusion.2 = (f32[512]{0:T(512)S(1)}, f32[1,128,512]{2,1,0:T(8,128)S(1)}) fusion(f32[512,1024]{1,0:T(8,128)S(1)} %get-tuple-element.18, f32[512,1024]{1,0:T(8,128)S(1)} %get-tuple-element.16, f32[512]{0:T(512)S(1)} %get-tuple-element.36, f32[512]{0:T(512)S(1)} %get-tuple-element.15, f32[]{:T(128)} %bitcast.11, f32[512]{0:T(512)S(1)} %get-tuple-element.35, ...), kind=kOutput, calls=%fused_computation.58 | convolution fusion | flops 138018304 | bytes 4728836 | tf_op jit(solution)/shard_map/hqk,khe->qhe/dot_general | solution.py:437
  53.4 0.3 fusion.14
  53.7 0.0 copy-start.4
  53.7 1.2 multiply_reduce_fusion.3
  54.9 0.0 copy-done.4
  54.9 0.1 fusion.16
  55.1 0.5 broadcast.183
  55.6 0.0 copy-start.2
  55.6 0.0 copy-start.3
  55.7 1.0 reduce.40
  56.7 0.3 copy.117
  56.9 0.9 reshape.311
  57.9 6.9 %all-to-all-start.1 = ((bf16[16,2,8192]{2,1,0:T(2,128)(2,1)}), bf16[16,2,8192]{2,1,0:T(2,128)(2,1)S(1)}, u32[]{:S(2)}, u32[]{:S(2)}) async-start(bf16[16,2,8192]{2,1,0:T(2,128)(2,1)} %reshape.311), calls=%async_computation.1 | async-start | bytes 1048576 | tf_op jit(solution)/shard_map/all_to_all | solution.py:443
  64.8 0.0 copy-done.2
  64.8 0.0 copy-done.3
  64.8 0.6 pad_maximum_fusion.1.meta_ref
  65.4 8.6 %all-to-all-done.1 = bf16[16,2,8192]{2,1,0:T(2,128)(2,1)S(1)} async-done(((bf16[16,2,8192]{2,1,0:T(2,128)(2,1)}), bf16[16,2,8192]{2,1,0:T(2,128)(2,1)S(1)}, u32[]{:S(2)}, u32[]{:S(2)}) %all-to-all-start.1) | async-done | bytes 524320 | tf_op jit(solution)/shard_map/all_to_all | solution.py:443
  74.1 0.5 reshape.312
  74.6 0.1 copy.113
  74.7 0.3 copy.112
  75.0 0.9 copy.116
  76.0 115.7 %experts.1 = bf16[128,2048]{1,0:T(8,128)(2,1)} custom-call(bf16[128,2048]{1,0:T(8,128)(2,1)} %bitcast.168, bf16[128,2048]{1,0:T(8,128)(2,1)} %bitcast.189, bf16[2048,2048]{1,0:T(8,128)(2,1)} %wo_hbm.1, f32[1,2048]{1,0:T(1,128)} %bitcast.190, f32[8,128]{1,0:T(8,128)} %pad_maximum_fusion.1.meta_ref, bf16[2048,1024]{1,0:T(8,128)(2,1)} %bitcast.165, ...), custom_call_target="tpu_custom_call" | custom-call | tf_op jit(solution)/shard_map/experts/pallas_call | solution.py:326
  191.7 1.9 copy.123
  (9 shorter events, 0.1 us)
Async XLA Ops:
  0.0 4.2 %copy-start.1 = (bf16[1,128,1024]{2,1,0:T(8,128)(2,1)S(1)}, bf16[1,128,1024]{2,1,0:T(8,128)(2,1)}, u32[]{:S(2)}) copy-start(bf16[1,128,1024]{2,1,0:T(8,128)(2,1)} %param.18) | copy-start | bytes 786436
  0.0 4.4 %copy-start = (bf16[1,128,2048]{2,1,0:T(8,128)(2,1)S(1)}, bf16[1,128,2048]{2,1,0:T(8,128)(2,1)}, u32[]{:S(2)}) copy-start(bf16[1,128,2048]{2,1,0:T(8,128)(2,1)} %param.19) | copy-start | bytes 1572868
  7.0 8.7 %copy-start.5 = (f32[16]{0:T(128)S(1)}, f32[16]{0:T(128)}, u32[]{:S(2)}) copy-start(f32[16]{0:T(128)} %param.20) | copy-start | bytes 196
  7.9 28.4 %all-to-all-start = ((bf16[128,16,384]{0,2,1:T(8,128)(2,1)}), bf16[128,16,384]{0,2,1:T(8,128)(2,1)S(1)}, u32[]{:S(2)}, u32[]{:S(2)}) async-start(bf16[128,16,384]{0,2,1:T(8,128)(2,1)} %constant_dynamic-update-slice_fusion), calls=%async_computation | async-start | bytes 3145728 | tf_op jit(solution)/shard_map/all_to_all | solution.py:368
  53.7 1.2 copy-start.4
  55.6 9.2 %copy-start.2 = (s32[1,128,4]{1,2,0:T(4,128)S(1)}, s32[1,128,4]{1,2,0:T(4,128)}, u32[]{:S(2)}) copy-start(s32[1,128,4]{1,2,0:T(4,128)} %param.25) | copy-start | bytes 6148
  55.6 9.2 %copy-start.3 = (f32[1,128,4]{1,2,0:T(4,128)S(1)}, f32[1,128,4]{1,2,0:T(4,128)}, u32[]{:S(2)}) copy-start(f32[1,128,4]{1,2,0:T(4,128)} %param.26) | copy-start | bytes 6148
  57.9 16.2 %all-to-all-start.1 = ((bf16[16,2,8192]{2,1,0:T(2,128)(2,1)}), bf16[16,2,8192]{2,1,0:T(2,128)(2,1)S(1)}, u32[]{:S(2)}, u32[]{:S(2)}) async-start(bf16[16,2,8192]{2,1,0:T(2,128)(2,1)} %reshape.311), calls=%async_computation.1 | async-start | bytes 1048576 | tf_op jit(solution)/shard_map/all_to_all | solution.py:443
where the time goes:
time: 196 us; the launch traced here: 194 us
  Pallas kernels  116 us (59%)
  waiting for transfers between devices  28.6 us (15%)
  local copies, waits for them, and re-layouts  14.8 us (8%)
  starting transfers between devices  14.8 us (8%)
  matrix products  13.9 us (7%)
  other arithmetic  5.55 us (3%)
    pallas_call x1, Pallas kernels, after_attention(): pl.pallas_call(moe_kernel, out_shape=jax.ShapeDtypeStruct((rows, width),...  116 us
    all_to_all x1, waiting for transfers between devices, sent_together(): lax.all_to_all(both, axis, split_axis=split_dim, concat_axis=concat_dim,...  20 us
    unnamed x27, local copies, waits for them, and re-layouts  11.6 us
    all_to_all x1, waiting for transfers between devices, on_device(): lax.all_to_all(head_out, 'sp', split_axis=0, concat_axis=1, tiled=True)  8.62 us
    dot_general x4, matrix products, on_device(): jnp.einsum('hqk,khe->qhe', mixture, value_head[:finish], preferred_elemen...  8.13 us
    all_to_all x1, starting transfers between devices, sent_together(): lax.all_to_all(both, axis, split_axis=split_dim, concat_axis=concat_dim,...  7.85 us
    all_to_all x1, starting transfers between devices, on_device(): lax.all_to_all(head_out, 'sp', split_axis=0, concat_axis=1, tiled=True)  6.95 us
  transfers between devices with their start and end apart: 2, of which 2 were waited for; matrix products, arithmetic and copies ran while one was open for 1% of the time, Pallas kernels for 0%

commit v1 on v0

--- a/solution.py
+++ b/solution.py
@@ -16,11 +16,14 @@
 CHUNKS = 4
 
 
-def moe_kernel(
-    head_ref, res_ref, wo_hbm, gain_ref, meta_ref, wg_hbm, wu_hbm, wd_hbm,
+def layer_kernel(
+    q1_hbm, k1_hbm, q2_hbm, k2_hbm, v_hbm, lambda_ref, hgain_ref,
+    res_ref, wo_hbm, gain_ref, meta_ref, wg_hbm, wu_hbm, wd_hbm,
     out_ref,
-    wg, wu, wd, nrm, mixed, gath, slab, xin, gacc, uacc, hid, back, rin,
+    q1, k1, q2, k2, vals, packed, keys, valt, hsend, head_ref,
+    wg, wu, wd, nrm, mixed, gath, slab, xin, acc, hid, back, rin,
     part_out, part_in, sum_out, sum_in, own, pick, wsel, meta,
+    lsem, as_, ar, hs, hr,
     wsem, meta_s, meta_r, xs, xr, cs, cr, ds, dr, bs, br, ps, pr, ts, tr,
 ):
     f32, bf16 = jnp.float32, jnp.bfloat16
@@ -58,6 +61,14 @@
     for i in range(1, ndp):
         pl.semaphore_signal(barrier, inc=1, device_id=(sp, (dp + i) % ndp), device_id_type=MESH)
 
+    loads = [
+        pltpu.make_async_copy(src, dst, lsem.at[i])
+        for i, (src, dst) in enumerate(
+            ((q1_hbm, q1), (q2_hbm, q2), (k1_hbm, k1), (k2_hbm, k2), (v_hbm, vals))
+        )
+    ]
+    for load in loads:
+        load.start()
     wo_a = pltpu.make_async_copy(wo_hbm.at[:, pl.ds(0, half)], wg, wsem.at[0])
     wo_b = pltpu.make_async_copy(wo_hbm.at[:, pl.ds(half, half)], wu, wsem.at[1])
     wd_c = pltpu.make_async_copy(wd_hbm, wd, wsem.at[2])
@@ -67,7 +78,29 @@
     wo_b.start()
     wd_c.start()
 
+    hd = q1.shape[1] // nsp
+    hv = vals.shape[1] // nsp
+    for load in loads:
+        load.wait()
+    for g in range(nsp // 2):
+        two = slice(g * 2 * hd, (g + 1) * 2 * hd)
+        for base, first, second in ((0, q1, q2), (2 * hd, k1, k2)):
+            a, b = first[:, two], second[:, two]
+            packed[2 * g, :, base : base + 2 * hd] = jnp.concatenate([a[:, :hd], b[:, :hd]], axis=1)
+            packed[2 * g + 1, :, base : base + 2 * hd] = jnp.concatenate(
+                [a[:, hd:], b[:, hd:]], axis=1
+            )
+    for h in range(nsp):
+        packed[h, :, 4 * hd :] = vals[:, h * hv : (h + 1) * hv]
+    keys[sp] = packed[sp]
+
     pl.semaphore_wait(barrier, nsp - 1 + ndp - 1)
+
+    def qkv(dst, src):
+        return remote(packed.at[dst], keys.at[src], as_.at[dst], ar.at[src], (dst, dp))
+
+    for i in range(nsp - 1):
+        qkv(peer(i), sp).start()
 
     def meta_copy(i, src):
         return remote(meta_ref, meta.at[src], meta_s.at[i], meta_r.at[i], (sp, (dp + i) % ndp))
@@ -75,6 +108,93 @@
     for i in range(1, ndp):
         meta_copy(i, dp).start()
     meta[dp] = meta_ref[...]
+
+    block = 2 * rows
+    blocks = nsp // 2
+    lam = lambda_ref[sp]
+    scale = hd ** (-0.5) * 1.4426950408889634
+
+    def heads(dst, src):
+        at = pl.ds(pl.multiple_of(src * hv, hv), hv)
+        return remote(hsend.at[dst], head_ref.at[:, at], hs.at[dst], hr.at[src], (dst, dp))
+
+    def folded(value, op):
+        return op(value.reshape(-1, 8, value.shape[1]), axis=0)
+
+    def attend(i, carry):
+        for half_block in range(2):
+            src = 2 * i + half_block
+
+            @pl.when(src != sp)
+            def _():
+                qkv(src, src).wait_recv()
+
+        pair = pl.ds(2 * i, 2)
+        turned = jnp.transpose(keys[pair, :, 4 * hd :].reshape(block, hv).astype(f32))
+        valt[:, pl.ds(pl.multiple_of(i * block, block), block)] = turned.astype(bf16)
+        query = keys[pair, :, : 2 * hd].reshape(block, 2 * hd)
+        lane = lax.broadcasted_iota(jnp.int32, (block, 2 * hd), 1)
+        zero = jnp.zeros_like(query)
+        both = jnp.concatenate(
+            [jnp.where(lane < hd, query, zero), jnp.where(lane < hd, zero, query)], axis=0
+        )
+
+        def score(j):
+            key = keys[pl.ds(2 * j, 2), :, 2 * hd : 4 * hd].reshape(block, 2 * hd)
+            return lax.dot_general(
+                key, both, (((1,), (1,)), ((), ())), preferred_element_type=f32
+            )
+
+        def at(j):
+            return pl.ds(pl.multiple_of(j * block, block), block)
+
+        def scores(j, top):
+            value = score(j)
+            acc[at(j), :] = value
+            return jnp.maximum(top, folded(value, jnp.max))
+
+        top = lax.fori_loop(0, i, scores, jnp.full((8, 2 * block), -1e30, f32))
+        below = lax.broadcasted_iota(jnp.int32, (block, block), 0)
+        seen = below <= lax.broadcasted_iota(jnp.int32, (block, block), 1)
+        value = jnp.where(jnp.concatenate([seen, seen], axis=1), score(i), -1e30)
+        acc[at(i), :] = value
+        top = jnp.maximum(top, folded(value, jnp.max))
+        top = jnp.max(top, axis=0, keepdims=True)
+
+        def powers(j, total):
+            value = jnp.exp2((acc[at(j), :] - top) * scale)
+            acc[at(j), :] = value
+            return total + folded(value, jnp.sum)
+
+        total = lax.fori_loop(0, i + 1, powers, jnp.zeros((8, 2 * block), f32))
+        total = jnp.sum(total, axis=0, keepdims=True)
+        first = 1.0 / total[:, :block]
+        second = lam / total[:, block:]
+
+        def values(j, raw):
+            mix = (acc[at(j), :block] * first - acc[at(j), block:] * second).astype(bf16)
+            return raw + jnp.dot(valt[:, at(j)], mix, preferred_element_type=f32)
+
+        raw = lax.fori_loop(0, i + 1, values, jnp.zeros((hv, block), f32))
+        size = lax.rsqrt(jnp.mean(raw * raw, axis=0, keepdims=True) + 1e-06)
+        done = (jnp.transpose(raw * size) * hgain_ref[...]).astype(bf16)
+        hsend[pair] = done.reshape(2, rows, hv)
+        for half_block in range(2):
+            dst = 2 * i + half_block
+
+            @pl.when(dst != sp)
+            def _():
+                heads(dst, sp).start()
+
+            @pl.when(dst == sp)
+            def _():
+                head_ref[:, pl.ds(pl.multiple_of(sp * hv, hv), hv)] = hsend[dst]
+
+        return carry
+
+    lax.fori_loop(0, blocks, attend, 0)
+    for i in range(nsp - 1):
+        heads(peer(i, -1), peer(i, -1)).wait_recv()
 
     tile = 256
     square = jnp.zeros((rows, 128), f32)
@@ -153,8 +273,9 @@
         return carry
 
     lax.fori_loop(0, ndp, table, 0)
-    gacc[...] = jnp.zeros_like(gacc)
-    uacc[...] = jnp.zeros_like(uacc)
+    acc[...] = jnp.zeros_like(acc)
+    filled = nsp * slots
+    span = acc.shape[1]
 
     def forward(k):
         for i in (0, 2, 1):
@@ -199,8 +320,12 @@
         def one(t, carry):
             at = pl.ds(pl.multiple_of(t * tile, tile), tile)
             taken = xin[:, :, cols(k)].reshape(nsp * slots, cw)
-            gacc[:, at] += jnp.dot(taken, wg[cols(k), at], preferred_element_type=f32)
-            uacc[:, at] += jnp.dot(taken, wu[cols(k), at], preferred_element_type=f32)
+            per = span // tile
+            to = pl.ds(pl.multiple_of((t % per) * tile, tile), tile)
+            low = pl.ds(pl.multiple_of((t // per) * filled, filled), filled)
+            high = pl.ds(pl.multiple_of((t // per + half // span) * filled, filled), filled)
+            acc[low, to] += jnp.dot(taken, wg[cols(k), at], preferred_element_type=f32)
+            acc[high, to] += jnp.dot(taken, wu[cols(k), at], preferred_element_type=f32)
             return carry
 
         lax.fori_loop(0, half // tile, one, 0)
@@ -231,9 +356,13 @@
 
     def unit(t, carry):
         at = pl.ds(pl.multiple_of(t * 32, 32), 32)
-        gate = jnp.minimum(gacc[at, :], 7.0)
-        upper = jnp.clip(uacc[at, :], -7.0, 7.0) + 1.0
-        hid[at, :] = (upper * gate / (1.0 + jnp.exp(-1.702 * gate))).astype(bf16)
+        for part_of in range(half // span):
+            low = pl.ds(pl.multiple_of(part_of * filled + t * 32, 32), 32)
+            high = pl.ds(pl.multiple_of((part_of + half // span) * filled + t * 32, 32), 32)
+            gate = jnp.minimum(acc[low, :], 7.0)
+            upper = jnp.clip(acc[high, :], -7.0, 7.0) + 1.0
+            made = upper * gate / (1.0 + jnp.exp(-1.702 * gate))
+            hid[at, part_of * span : (part_of + 1) * span] = made.astype(bf16)
         return carry
 
     lax.fori_loop(0, nsp * slots // 32, unit, 0)
@@ -296,6 +425,9 @@
     lax.fori_loop(0, n, combine, 0)
     finish(n - 1)
 
+    for i in range(nsp - 1):
+        qkv(peer(i), sp).wait_send()
+        heads(peer(i), sp).wait_send()
     for i in range(1, ndp):
         meta_copy(i, dp).wait_send()
 
@@ -312,61 +444,6 @@
         return carry
 
     lax.fori_loop(0, n, drain, 0)
-
-
-def after_attention(heads_out, residual, out_weight, norm_gain, meta, gate_weight, up_weight, down_weight, nsp, ndp):
-    rows, width = residual.shape
-    hidden = gate_weight.shape[1]
-    slots = CAP * ndp
-    n = CHUNKS
-    bf16, f32 = jnp.bfloat16, jnp.float32
-    vmem = pl.BlockSpec(memory_space=pltpu.VMEM)
-    hbm = pl.BlockSpec(memory_space=pl.ANY)
-    dma = pltpu.SemaphoreType.DMA
-    return pl.pallas_call(
-        moe_kernel,
-        out_shape=jax.ShapeDtypeStruct((rows, width), bf16),
-        in_specs=[vmem, vmem, hbm, vmem, vmem, hbm, hbm, hbm],
-        out_specs=vmem,
-        scratch_shapes=[
-            pltpu.VMEM((width, hidden), bf16),
-            pltpu.VMEM((width, hidden), bf16),
-            pltpu.VMEM((hidden, width), bf16),
-            pltpu.VMEM((rows, width), bf16),
-            pltpu.VMEM((rows, width), f32),
-            pltpu.VMEM((ndp, rows, width), bf16),
-            pltpu.VMEM((nsp, slots, width), bf16),
-            pltpu.VMEM((nsp, slots, width), bf16),
-            pltpu.VMEM((nsp * slots, hidden), f32),
-            pltpu.VMEM((nsp * slots, hidden), f32),
-            pltpu.VMEM((nsp * slots, hidden), bf16),
-            pltpu.VMEM((nsp, slots, width), bf16),
-            pltpu.VMEM((nsp, slots, width), bf16),
-            pltpu.VMEM((RING, rows, width), bf16),
-            pltpu.VMEM((RING, rows, width), bf16),
-            pltpu.VMEM((RING, rows, width), bf16),
-            pltpu.VMEM((RING, rows, width), bf16),
-            pltpu.VMEM((RING, rows, width // n), f32),
-            pltpu.VMEM((nsp * slots, ndp * rows), bf16),
-            pltpu.VMEM((ndp, rows, nsp * slots), bf16),
-            pltpu.VMEM((ndp, 8, rows), f32),
-            dma((5,)), dma((ndp,)), dma((ndp,)),
-            dma((n, 3)), dma((n, 3)), dma((n, 4)), dma((n, 4)),
-            dma((n, nsp)), dma((n, nsp)), dma((n, nsp)), dma((n, nsp)),
-            dma((n,)), dma((n,)), dma((n, 3)), dma((n, 3)),
-        ],
-        compiler_params=pltpu.CompilerParams(
-            collective_id=1, has_side_effects=True, vmem_limit_bytes=64 * 1000 * 1000
-        ),
-        name="experts",
-    )(heads_out, residual, out_weight, norm_gain[None, :], meta, gate_weight, up_weight, down_weight)
-
-
-def sent_together(arrays, axis, split_dim, concat_dim, along):
-    widths = [a.shape[along] for a in arrays]
-    both = jnp.concatenate(arrays, axis=along)
-    out = lax.all_to_all(both, axis, split_axis=split_dim, concat_axis=concat_dim, tiled=True)
-    return tuple(jnp.split(out, [sum(widths[:k]) for k in range(1, len(widths))], axis=along))
 
 
 def on_device(
@@ -386,73 +463,70 @@
     up_weight,
     down_weight,
 ):
-    tok_rows = query_first.shape[1]
-    heads = mix_lambda.shape[0]
-    query_one, key_one, query_two, key_two, value_head = sent_together(
-        (
-            query_first[0].reshape(tok_rows, heads, -1),
-            key_first[0].reshape(tok_rows, heads, -1),
-            query_second[0].reshape(tok_rows, heads, -1),
-            key_second[0].reshape(tok_rows, heads, -1),
-            value_rows[0].reshape(tok_rows, heads, -1),
+    nsp, ndp = lax.axis_size("sp"), lax.axis_size("dp")
+    rows, width = residual.shape[1:]
+    hidden = gate_weight.shape[2]
+    qk = query_first.shape[2]
+    hv = head_gain.shape[0]
+    packed = 4 * qk // nsp + hv
+    slots = CAP * ndp
+    n = CHUNKS
+    bf16, f32 = jnp.bfloat16, jnp.float32
+    meta = jnp.concatenate([routes[0].T.astype(f32), route_weights[0].T], axis=0)
+    vmem = pl.BlockSpec(memory_space=pltpu.VMEM)
+    smem = pl.BlockSpec(memory_space=pltpu.SMEM)
+    hbm = pl.BlockSpec(memory_space=pl.ANY)
+    dma = pltpu.SemaphoreType.DMA
+    out = pl.pallas_call(
+        layer_kernel,
+        out_shape=jax.ShapeDtypeStruct((rows, width), bf16),
+        in_specs=[hbm] * 5 + [smem, vmem, vmem, hbm, vmem, vmem, hbm, hbm, hbm],
+        out_specs=vmem,
+        scratch_shapes=[
+            pltpu.VMEM((rows, qk), bf16),
+            pltpu.VMEM((rows, qk), bf16),
+            pltpu.VMEM((rows, qk), bf16),
+            pltpu.VMEM((rows, qk), bf16),
+            pltpu.VMEM((rows, nsp * hv), bf16),
+            pltpu.VMEM((nsp, rows, packed), bf16),
+            pltpu.VMEM((nsp, rows, packed), bf16),
+            pltpu.VMEM((hv, nsp * rows), bf16),
+            pltpu.VMEM((nsp, rows, hv), bf16),
+            pltpu.VMEM((rows, nsp * hv), bf16),
+            pltpu.VMEM((width, hidden), bf16),
+            pltpu.VMEM((width, hidden), bf16),
+            pltpu.VMEM((hidden, width), bf16),
+            pltpu.VMEM((rows, width), bf16),
+            pltpu.VMEM((rows, width), f32),
+            pltpu.VMEM((ndp, rows, width), bf16),
+            pltpu.VMEM((nsp, slots, width), bf16),
+            pltpu.VMEM((nsp, slots, width), bf16),
+            pltpu.VMEM((4 * nsp * slots, hidden // 2), f32),
+            pltpu.VMEM((nsp * slots, hidden), bf16),
+            pltpu.VMEM((nsp, slots, width), bf16),
+            pltpu.VMEM((nsp, slots, width), bf16),
+            pltpu.VMEM((RING, rows, width), bf16),
+            pltpu.VMEM((RING, rows, width), bf16),
+            pltpu.VMEM((RING, rows, width), bf16),
+            pltpu.VMEM((RING, rows, width), bf16),
+            pltpu.VMEM((RING, rows, width // n), f32),
+            pltpu.VMEM((nsp * slots, ndp * rows), bf16),
+            pltpu.VMEM((ndp, rows, nsp * slots), bf16),
+            pltpu.VMEM((ndp, 8, rows), f32),
+            dma((5,)), dma((nsp,)), dma((nsp,)), dma((nsp,)), dma((nsp,)),
+            dma((5,)), dma((ndp,)), dma((ndp,)),
+            dma((n, 3)), dma((n, 3)), dma((n, 4)), dma((n, 4)),
+            dma((n, nsp)), dma((n, nsp)), dma((n, nsp)), dma((n, nsp)),
+            dma((n,)), dma((n,)), dma((n, 3)), dma((n, 3)),
+        ],
+        compiler_params=pltpu.CompilerParams(
+            collective_id=1, has_side_effects=True, vmem_limit_bytes=67000000
         ),
-        "sp",
-        1,
-        0,
-        2,
-    )
-    length = query_one.shape[0]
-    local = query_one.shape[1]
-    value_width = value_head.shape[2]
-    scale = query_one.shape[2] ** (-0.5)
-    first_head = lax.axis_index("sp") * local
-    weight_two = lax.dynamic_slice_in_dim(mix_lambda, first_head, local)[:, None, None]
-    qblock = min(length, max(512, length // 16))
-    outputs = []
-    for step in range(length // qblock):
-        begin = step * qblock
-        finish = begin + qblock
-        score_one = (
-            jnp.einsum(
-                "qhd,khd->hqk",
-                query_one[begin:finish],
-                key_one[:finish],
-                preferred_element_type=jnp.float32,
-            )
-            * scale
-        )
-        score_two = (
-            jnp.einsum(
-                "qhd,khd->hqk",
-                query_two[begin:finish],
-                key_two[:finish],
-                preferred_element_type=jnp.float32,
-            )
-            * scale
-        )
-        visible = jnp.arange(finish)[None, :] <= (begin + jnp.arange(qblock))[:, None]
-        prob_one = jax.nn.softmax(jnp.where(visible[None], score_one, -1e30), axis=-1)
-        prob_two = jax.nn.softmax(jnp.where(visible[None], score_two, -1e30), axis=-1)
-        mixture = (prob_one - weight_two * prob_two).astype(jnp.bfloat16)
-        head_raw = jnp.einsum(
-            "hqk,khe->qhe", mixture, value_head[:finish], preferred_element_type=jnp.float32
-        )
-        factor = lax.rsqrt(jnp.mean(head_raw * head_raw, axis=-1, keepdims=True) + 1e-06)
-        outputs.append((head_raw * factor * head_gain).astype(jnp.bfloat16))
-    head_out = jnp.concatenate(outputs, axis=0)
-    returned = lax.all_to_all(head_out, "sp", split_axis=0, concat_axis=1, tiled=True)
-    meta = jnp.concatenate([routes[0].T.astype(jnp.float32), route_weights[0].T], axis=0)
-    out = after_attention(
-        returned.reshape(tok_rows, heads * value_width),
-        residual[0],
-        out_weight,
-        norm_gain,
-        meta,
-        gate_weight[0],
-        up_weight[0],
-        down_weight[0],
-        lax.axis_size("sp"),
-        lax.axis_size("dp"),
+        name="layer",
+    )(
+        query_first[0], key_first[0], query_second[0], key_second[0], value_rows[0],
+        mix_lambda, head_gain[None, :], residual[0], out_weight, norm_gain[None, :], meta,
+        gate_weight[0], up_weight[0], down_weight[0],
     )
     return out[None]
 

time: 196 us -> 173 us (0.88); the launches traced: 194 us -> 173 us
  Pallas kernels: 116 us -> 169 us
  waiting for transfers between devices: 28.6 us -> 0 us
  starting transfers between devices: 14.8 us -> 0 us
  matrix products: 13.9 us -> 0 us
  local copies, waits for them, and re-layouts: 14.8 us -> 1.88 us
  other arithmetic: 5.55 us -> 1.96 us
    pallas_call x1, Pallas kernels: 116 us -> 169 us  [on_device(): pl.pallas_call(layer_kernel, out_shape=jax.ShapeDtypeStruct((rows, width)...]
    all_to_all x2 -> x0, waiting for transfers between devices: 28.6 us -> none  [the longest x1 20 us: sent_together(): lax.all_to_all(both, axis, split_axis=split_dim, concat_axis=concat_dim,...]
    all_to_all x2 -> x0, starting transfers between devices: 14.8 us -> none  [the longest x1 7.85 us: sent_together(): lax.all_to_all(both, axis, split_axis=split_dim, concat_axis=concat_dim,...]
    dot_general x12 -> x0, matrix products: 13.9 us -> none  [the longest x4 8.13 us: on_device(): jnp.einsum('hqk,khe->qhe', mixture, value_head[:finish], preferred_elemen...]
    unnamed x27 -> x1, local copies, waits for them, and re-layouts: 11.6 us -> 1.88 us
    reduce_sum x4 -> x0, other arithmetic: 3.7 us -> none  [on_device(): jax.nn.softmax(jnp.where(visible[None], score_one, -1e+30), axis=-1)]
  transfers between devices with their start and end apart: 2 -> 0, of which waited for: 2 -> 0; matrix products, arithmetic and copies ran while one was open for 1% -> 0% of each run, Pallas kernels for 0% -> 0%
where the time goes in v1:
time: 173 us
  Pallas kernels  169 us (98%)
  other arithmetic  1.96 us (1%)
  local copies, waits for them, and re-layouts  1.88 us (1%)
    pallas_call x1, Pallas kernels, on_device(): pl.pallas_call(layer_kernel, out_shape=jax.ShapeDtypeStruct((rows, width)...  169 us

profile of v1, /device:TPU:9, one launch (start us, length us, event | category | flops | bytes accessed | tf_op | source)
XLA Modules:
  0.0 173.0 jit_solution(3118308647472858390)
XLA Ops:
  0.0 0.7 convert_bitcast_fusion
  0.7 1.3 pad_maximum_fusion.meta_ref
  2.0 169.2 %layer.1 = bf16[128,2048]{1,0:T(8,128)(2,1)} custom-call(bf16[128,1024]{1,0:T(8,128)(2,1)} %bitcast.25, bf16[128,1024]{1,0:T(8,128)(2,1)} %bitcast.26, bf16[128,1024]{1,0:T(8,128)(2,1)} %bitcast.27, bf16[128,1024]{1,0:T(8,128)(2,1)} %bitcast.28, bf16[128,2048]{1,0:T(8,128)(2,1)} %bitcast.23, f32[16]{0:T(128)} %lambda_ref.1, f32[1,128]{1,0:T(1,128)} %bitcast.31, ...), custom_call_target="tpu_custom_call" | custom-call | tf_op jit(solution)/shard_map/layer/pallas_call | solution.py:480
  171.2 1.9 %copy.17 = bf16[1,128,2048]{2,1,0:T(8,128)(2,1)} copy(bf16[1,128,2048]{2,1,0:T(8,128)(2,1)} %bitcast.22) | data formatting | bytes 1048576

commit v2 on v1

--- a/solution.py
+++ b/solution.py
@@ -13,14 +13,14 @@
     (0, 1), (1, 0), (0, 3), (3, 0), (1, 1), (3, 3), (1, 3), (3, 1),
     (0, 2), (2, 0), (1, 2), (2, 1), (3, 2), (2, 3), (2, 2),
 )
-CHUNKS = 4
+CHUNKS = 8
 
 
 def layer_kernel(
     q1_hbm, k1_hbm, q2_hbm, k2_hbm, v_hbm, lambda_ref, hgain_ref,
     res_ref, wo_hbm, gain_ref, meta_ref, wg_hbm, wu_hbm, wd_hbm,
     out_ref,
-    q1, k1, q2, k2, vals, packed, keys, valt, hsend, head_ref,
+    q1, k1, q2, k2, vals, packed, keys, valt, mix, hsend, head_ref,
     wg, wu, wd, nrm, mixed, gath, slab, xin, acc, hid, back, rin,
     part_out, part_in, sum_out, sum_in, own, pick, wsel, meta,
     lsem, as_, ar, hs, hr,
@@ -74,14 +74,14 @@
     wd_c = pltpu.make_async_copy(wd_hbm, wd, wsem.at[2])
     wg_c = pltpu.make_async_copy(wg_hbm, wg, wsem.at[3])
     wu_c = pltpu.make_async_copy(wu_hbm, wu, wsem.at[4])
-    wo_a.start()
-    wo_b.start()
-    wd_c.start()
 
     hd = q1.shape[1] // nsp
     hv = vals.shape[1] // nsp
     for load in loads:
         load.wait()
+    wo_a.start()
+    wo_b.start()
+    wd_c.start()
     for g in range(nsp // 2):
         two = slice(g * 2 * hd, (g + 1) * 2 * hd)
         for base, first, second in ((0, q1, q2), (2 * hd, k1, k2)):
@@ -96,11 +96,16 @@
 
     pl.semaphore_wait(barrier, nsp - 1 + ndp - 1)
 
-    def qkv(dst, src):
-        return remote(packed.at[dst], keys.at[src], as_.at[dst], ar.at[src], (dst, dp))
-
-    for i in range(nsp - 1):
-        qkv(peer(i), sp).start()
+    def qkv(dst, src, which):
+        at = pl.ds(0, 4 * hd) if which == 0 else pl.ds(4 * hd, hv)
+        return remote(
+            packed.at[dst, :, at], keys.at[src, :, at], as_.at[which, dst], ar.at[which, src],
+            (dst, dp),
+        )
+
+    for which in range(2):
+        for i in range(nsp - 1):
+            qkv(peer(i), sp, which).start()
 
     def meta_copy(i, src):
         return remote(meta_ref, meta.at[src], meta_s.at[i], meta_r.at[i], (sp, (dp + i) % ndp))
@@ -121,44 +126,38 @@
     def folded(value, op):
         return op(value.reshape(-1, 8, value.shape[1]), axis=0)
 
-    def attend(i, carry):
-        for half_block in range(2):
-            src = 2 * i + half_block
+    def at(j):
+        return pl.ds(pl.multiple_of(j * block, block), block)
+
+    def arrived(i, which):
+        for src in (2 * i, 2 * i + 1):
 
             @pl.when(src != sp)
             def _():
-                qkv(src, src).wait_recv()
-
-        pair = pl.ds(2 * i, 2)
-        turned = jnp.transpose(keys[pair, :, 4 * hd :].reshape(block, hv).astype(f32))
-        valt[:, pl.ds(pl.multiple_of(i * block, block), block)] = turned.astype(bf16)
-        query = keys[pair, :, : 2 * hd].reshape(block, 2 * hd)
-        lane = lax.broadcasted_iota(jnp.int32, (block, 2 * hd), 1)
+                qkv(src, src, which).wait_recv()
+
+    below = lax.broadcasted_iota(jnp.int32, (block, 2 * block), 0)
+    across = lax.broadcasted_iota(jnp.int32, (block, 2 * block), 1)
+    seen = below <= jnp.where(across < block, across, across - block)
+    lane = lax.broadcasted_iota(jnp.int32, (block, 2 * hd), 1)
+
+    def attend(i):
+        arrived(i, 0)
+        query = keys[2 * i : 2 * i + 2, :, : 2 * hd].reshape(block, 2 * hd)
         zero = jnp.zeros_like(query)
         both = jnp.concatenate(
             [jnp.where(lane < hd, query, zero), jnp.where(lane < hd, zero, query)], axis=0
         )
-
-        def score(j):
-            key = keys[pl.ds(2 * j, 2), :, 2 * hd : 4 * hd].reshape(block, 2 * hd)
-            return lax.dot_general(
+        top = jnp.full((8, 2 * block), -1e30, f32)
+        for j in range(i + 1):
+            key = keys[2 * j : 2 * j + 2, :, 2 * hd : 4 * hd].reshape(block, 2 * hd)
+            value = lax.dot_general(
                 key, both, (((1,), (1,)), ((), ())), preferred_element_type=f32
             )
-
-        def at(j):
-            return pl.ds(pl.multiple_of(j * block, block), block)
-
-        def scores(j, top):
-            value = score(j)
-            acc[at(j), :] = value
-            return jnp.maximum(top, folded(value, jnp.max))
-
-        top = lax.fori_loop(0, i, scores, jnp.full((8, 2 * block), -1e30, f32))
-        below = lax.broadcasted_iota(jnp.int32, (block, block), 0)
-        seen = below <= lax.broadcasted_iota(jnp.int32, (block, block), 1)
-        value = jnp.where(jnp.concatenate([seen, seen], axis=1), score(i), -1e30)
-        acc[at(i), :] = value
-        top = jnp.maximum(top, folded(value, jnp.max))
+            if j == i:
+                value = jnp.where(seen, value, -1e30)
+            acc[j * block : (j + 1) * block, :] = value
+            top = jnp.maximum(top, folded(value, jnp.max))
         top = jnp.max(top, axis=0, keepdims=True)
 
         def powers(j, total):
@@ -171,16 +170,24 @@
         first = 1.0 / total[:, :block]
         second = lam / total[:, block:]
 
-        def values(j, raw):
-            mix = (acc[at(j), :block] * first - acc[at(j), block:] * second).astype(bf16)
-            return raw + jnp.dot(valt[:, at(j)], mix, preferred_element_type=f32)
-
-        raw = lax.fori_loop(0, i + 1, values, jnp.zeros((hv, block), f32))
+        def mixed_up(j, carry):
+            value = acc[at(j), :block] * first - acc[at(j), block:] * second
+            mix[i * (i + 1) // 2 + j] = value.astype(bf16)
+            return carry
+
+        lax.fori_loop(0, i + 1, mixed_up, 0)
+
+    def gather_values(i):
+        arrived(i, 1)
+        turned = jnp.transpose(keys[2 * i : 2 * i + 2, :, 4 * hd :].reshape(block, hv).astype(f32))
+        valt[:, i * block : (i + 1) * block] = turned.astype(bf16)
+        begin = i * (i + 1) // 2
+        taken = mix[begin : begin + i + 1].reshape((i + 1) * block, block)
+        raw = jnp.dot(valt[:, : (i + 1) * block], taken, preferred_element_type=f32)
         size = lax.rsqrt(jnp.mean(raw * raw, axis=0, keepdims=True) + 1e-06)
         done = (jnp.transpose(raw * size) * hgain_ref[...]).astype(bf16)
-        hsend[pair] = done.reshape(2, rows, hv)
-        for half_block in range(2):
-            dst = 2 * i + half_block
+        hsend[2 * i : 2 * i + 2] = done.reshape(2, rows, hv)
+        for dst in (2 * i, 2 * i + 1):
 
             @pl.when(dst != sp)
             def _():
@@ -190,9 +197,10 @@
             def _():
                 head_ref[:, pl.ds(pl.multiple_of(sp * hv, hv), hv)] = hsend[dst]
 
-        return carry
-
-    lax.fori_loop(0, blocks, attend, 0)
+    for i in range(blocks):
+        attend(i)
+    for i in range(blocks):
+        gather_values(i)
     for i in range(nsp - 1):
         heads(peer(i, -1), peer(i, -1)).wait_recv()
 
@@ -330,29 +338,21 @@
 
         lax.fori_loop(0, half // tile, one, 0)
 
-    forward(0)
-
     def dispatch(k, carry):
+        forward(k)
         build(k)
         send_all(slab, xin, ds, dr, k)
-
-        @pl.when(k + 1 < n)
-        def _():
-            forward(k + 1)
-
-        @pl.when(k == 1)
-        def _():
-            wg_c.wait()
-            wu_c.wait()
-
-        @pl.when(k > 0)
-        def _():
-            expert_in(k - 1)
-
         return carry
 
     lax.fori_loop(0, n, dispatch, 0)
-    expert_in(n - 1)
+    wg_c.wait()
+    wu_c.wait()
+
+    def receive(k, carry):
+        expert_in(k)
+        return carry
+
+    lax.fori_loop(0, n, receive, 0)
 
     def unit(t, carry):
         at = pl.ds(pl.multiple_of(t * 32, 32), 32)
@@ -426,7 +426,8 @@
     finish(n - 1)
 
     for i in range(nsp - 1):
-        qkv(peer(i), sp).wait_send()
+        qkv(peer(i), sp, 0).wait_send()
+        qkv(peer(i), sp, 1).wait_send()
         heads(peer(i), sp).wait_send()
     for i in range(1, ndp):
         meta_copy(i, dp).wait_send()
@@ -491,6 +492,7 @@
             pltpu.VMEM((nsp, rows, packed), bf16),
             pltpu.VMEM((nsp, rows, packed), bf16),
             pltpu.VMEM((hv, nsp * rows), bf16),
+            pltpu.VMEM((nsp * (nsp + 2) // 8, 2 * rows, 2 * rows), bf16),
             pltpu.VMEM((nsp, rows, hv), bf16),
             pltpu.VMEM((rows, nsp * hv), bf16),
             pltpu.VMEM((width, hidden), bf16),
@@ -513,7 +515,7 @@
             pltpu.VMEM((nsp * slots, ndp * rows), bf16),
             pltpu.VMEM((ndp, rows, nsp * slots), bf16),
             pltpu.VMEM((ndp, 8, rows), f32),
-            dma((5,)), dma((nsp,)), dma((nsp,)), dma((nsp,)), dma((nsp,)),
+            dma((5,)), dma((2, nsp)), dma((2, nsp)), dma((nsp,)), dma((nsp,)),
             dma((5,)), dma((ndp,)), dma((ndp,)),
             dma((n, 3)), dma((n, 3)), dma((n, 4)), dma((n, 4)),
             dma((n, nsp)), dma((n, nsp)), dma((n, nsp)), dma((n, nsp)),

time: 173 us -> 149 us (0.86); the launches traced: 173 us -> 147 us
  Pallas kernels: 169 us -> 143 us
    pallas_call x1, Pallas kernels: 169 us -> 143 us  [on_device(): pl.pallas_call(layer_kernel, out_shape=jax.ShapeDtypeStruct((rows, width)...]
where the time goes in v2:
time: 149 us; the launch traced here: 147 us
  Pallas kernels  143 us (96%)
  other arithmetic  1.96 us (1%)
  local copies, waits for them, and re-layouts  1.88 us (1%)
    pallas_call x1, Pallas kernels, on_device(): pl.pallas_call(layer_kernel, out_shape=jax.ShapeDtypeStruct((rows, width)...  143 us

profile of v2, /device:TPU:9, one launch (start us, length us, event | category | flops | bytes accessed | tf_op | source)
XLA Modules:
  0.0 147.0 jit_solution(6583303661412107905)
XLA Ops:
  0.0 0.7 convert_bitcast_fusion
  0.7 1.3 pad_maximum_fusion.meta_ref
  2.0 143.2 %layer.1 = bf16[128,2048]{1,0:T(8,128)(2,1)} custom-call(bf16[128,1024]{1,0:T(8,128)(2,1)} %bitcast.25, bf16[128,1024]{1,0:T(8,128)(2,1)} %bitcast.26, bf16[128,1024]{1,0:T(8,128)(2,1)} %bitcast.27, bf16[128,1024]{1,0:T(8,128)(2,1)} %bitcast.28, bf16[128,2048]{1,0:T(8,128)(2,1)} %bitcast.23, f32[16]{0:T(128)} %lambda_ref.1, f32[1,128]{1,0:T(1,128)} %bitcast.31, ...), custom_call_target="tpu_custom_call" | custom-call | tf_op jit(solution)/shard_map/layer/pallas_call | solution.py:481
  145.2 1.9 %copy.17 = bf16[1,128,2048]{2,1,0:T(8,128)(2,1)} copy(bf16[1,128,2048]{2,1,0:T(8,128)(2,1)} %bitcast.22) | data formatting | bytes 1048576
